TPU v7x, 32 devices: a whole 2x2x4 slice. The times are simulated.
32 devices in a mesh: sp: 8 (over z, x), tp: 4 (over y, core).
Axes of the slice: x: 2, y: 2, z: 4, core: 2. Of those that a mesh axis runs over, the one named last changes fastest.
Arguments:
- residual: bfloat16 [3072, 2048], P('sp', 'tp'), may hold values from -6 to 6
- query_nope: bfloat16 [3072, 4096], P('sp', 'tp'), may hold values from -9 to 9
- query_rope: bfloat16 [3072, 2048], P('sp', 'tp'), may hold values from -600 to 600
- latent: bfloat16 [3072, 512], P('sp'), may hold values from -6 to 6
- rope_key: bfloat16 [3072, 64], P('sp'), may hold values from -6 to 6
- doc_ids: int32 [3072], P('sp'), may hold values from 0 to 3, never falling along the last dimension, each value on 1 to 1152 neighbouring positions
- key_up: bfloat16 [512, 4096], P(None, 'tp'), may hold values from -0.25 to 0.25
- value_up: bfloat16 [512, 4096], P(None, 'tp'), may hold values from -0.25 to 0.25
- out_proj: bfloat16 [4096, 2048], P('tp'), may hold values from -0.375 to 0.375
- norm1_gain: bfloat16 [2048], P('tp'), may hold values from 0.099609375 to 1.8984375
- norm1_bias: bfloat16 [2048], P('tp'), may hold values from -3 to 3
- ffn_gate: bfloat16 [2048, 5632], P('sp', 'tp'), may hold values from -0.125 to 0.125
- ffn_value: bfloat16 [2048, 5632], P('sp', 'tp'), may hold values from -0.125 to 0.125
- conv_gate: bfloat16 [3, 5632], P(None, 'tp'), may hold values from -3.5 to 3.5
- conv_value: bfloat16 [3, 5632], P(None, 'tp'), may hold values from -3.5 to 3.5
- ffn_down: bfloat16 [5632, 2048], P('tp', 'sp'), may hold values from -0.15625 to 0.15625
- norm2_gain: bfloat16 [2048], P('tp'), may hold values from 0.099609375 to 1.8984375
- norm2_bias: bfloat16 [2048], P('tp'), may hold values from -3 to 3
Outputs:
- layer_out: bfloat16 [3072, 2048], P('sp', 'tp')
Inputs may be any that keep to these rules, and one draw needn't show every extreme that they name: `doc_ids`: document numbers never fall along the positions; each document holds 1 to 1152 positions, and one holds exactly 1152.
All inputs are finite; a program needn't handle non-finite values.
Results may differ from a plain program's by a relative error of at most 0.014.
Values may be sent and summed in bfloat16 or wider, within the bound.
A program may use at most 128 MiB of HBM per device.

v0:
```python
import jax
import jax.numpy as jnp
from jax import lax
from jax.sharding import PartitionSpec as P

D = 2048
NOPE = 128
ROPE = 64
VDIM = 128
CONV = 3
REACH = 3
norm_eps = 1e-05
residual_scale = 8.0**0.25
rope_base_freq = 10000.0
masked_score = -1e30


def passed_along(value, axis, by):
    count = lax.axis_size(axis)
    pairs = [(i, i + by) for i in range(count) if 0 <= i + by < count]
    return lax.ppermute(value, axis, pairs)


def tables(positions):
    frequencies = 1.0 / rope_base_freq ** (jnp.arange(0, ROPE, 2, dtype=jnp.float32) / ROPE)
    angles = positions.astype(jnp.float32)[:, None] * frequencies[None, :]
    return (jnp.cos(angles), jnp.sin(angles))


def rotate(vectors, cosine, sine_table):
    half_width = vectors.shape[-1] // 2
    front_half = vectors[..., :half_width]
    back_half = vectors[..., half_width:]
    return jnp.concatenate(
        [
            front_half * cosine - back_half * sine_table,
            front_half * sine_table + back_half * cosine,
        ],
        axis=-1,
    )


def scatter_sum(terms, axis):
    count = lax.axis_size(axis)
    width = terms.shape[1] // count
    parts = jnp.stack([terms[:, i * width : (i + 1) * width] for i in range(count)])
    got = lax.all_to_all(parts.astype(jnp.bfloat16), axis, 0, 0)
    return jnp.sum(got.astype(jnp.float32), 0)


def finish(mixed, totals, gain_row, bias_row):
    row_mean = totals[0][:, None] / D
    row_power = totals[1][:, None] / D
    return (mixed - row_mean) * lax.rsqrt(
        row_power - row_mean * row_mean + norm_eps
    ) * gain_row.astype(jnp.float32) + bias_row.astype(jnp.float32)


def local(
    residual,
    query_nope,
    query_rope,
    latent,
    rope_key,
    doc_ids,
    key_up,
    value_up,
    out_proj,
    norm1_gain,
    norm1_bias,
    ffn_gate,
    ffn_value,
    conv_gate,
    conv_value,
    ffn_down,
    norm2_gain,
    norm2_bias,
):
    row_count = latent.shape[0]
    head_count = query_nope.shape[1] // NOPE
    local_units = ffn_gate.shape[1]
    rim_rows = CONV - 1
    whole_gate, whole_value, whole_down = (
        lax.all_gather(ffn_gate, "sp", axis=0, tiled=True),
        lax.all_gather(ffn_value, "sp", axis=0, tiled=True),
        lax.all_gather(ffn_down, "sp", axis=1, tiled=True),
    )
    offset = lax.axis_index("sp") * row_count
    positions = offset + jnp.arange(row_count, dtype=jnp.int32)
    cosine, sine_table = tables(positions)
    turned_key = rotate(rope_key.astype(jnp.float32), cosine, sine_table).astype(jnp.bfloat16)
    turned_query = rotate(
        query_rope.astype(jnp.float32).reshape(row_count, head_count, ROPE),
        cosine[:, None],
        sine_table[:, None],
    ).astype(jnp.bfloat16)
    latent_list = []
    rim_list = []
    doc_list = []
    for shift_step in range(REACH, 0, -1):
        far_latent, far_key, far_doc = passed_along((latent, turned_key, doc_ids), "sp", shift_step)
        latent_list.append(far_latent)
        rim_list.append(far_key)
        doc_list.append(far_doc)
    win_latent = jnp.concatenate(latent_list + [latent], 0)
    win_key = jnp.concatenate(rim_list + [turned_key], 0)
    win_doc = jnp.concatenate(doc_list + [doc_ids], 0)
    key_rows = jnp.dot(win_latent, key_up, preferred_element_type=jnp.float32).astype(jnp.bfloat16)
    values = jnp.dot(win_latent, value_up, preferred_element_type=jnp.float32).astype(jnp.bfloat16)
    window = key_rows.shape[0]
    key_pos = offset - REACH * row_count + jnp.arange(window, dtype=jnp.int32)
    allowed = (
        (key_pos[None, :] <= positions[:, None])
        & (key_pos[None, :] >= 0)
        & (win_doc[None, :] == doc_ids[:, None])
    )
    scale = (NOPE + ROPE) ** (-0.5)
    scores = jnp.einsum(
        "qhd,khd->hqk",
        query_nope.reshape(row_count, head_count, NOPE),
        key_rows.reshape(window, head_count, NOPE),
        preferred_element_type=jnp.float32,
    )
    scores = scores + jnp.einsum(
        "qhr,kr->hqk", turned_query, win_key, preferred_element_type=jnp.float32
    )
    scores = jnp.where(allowed[None], scores * scale, masked_score)
    row_max = jnp.max(scores, -1, keepdims=True)
    weights = jnp.exp(scores - row_max)
    weights = (weights / jnp.sum(weights, -1, keepdims=True)).astype(jnp.bfloat16)
    attended = jnp.einsum(
        "hqk,khd->qhd",
        weights,
        values.reshape(window, head_count, VDIM),
        preferred_element_type=jnp.float32,
    )
    attended = attended.astype(jnp.bfloat16).reshape(row_count, head_count * VDIM)
    head_terms = jnp.dot(attended, out_proj, preferred_element_type=jnp.float32)
    projected = scatter_sum(head_terms, "tp")
    mixed_one = residual_scale * residual.astype(jnp.float32) + projected
    totals_one = lax.psum((jnp.sum(mixed_one, 1), jnp.sum(mixed_one * mixed_one, 1)), "tp")
    normed = finish(mixed_one, totals_one, norm1_gain, norm1_bias).astype(jnp.bfloat16)
    half = row_count // 2
    full_rows = jnp.concatenate(
        [
            lax.all_gather(normed[:half], "tp", axis=1, tiled=True),
            lax.all_gather(normed[half:], "tp", axis=1, tiled=True),
        ],
        0,
    )
    gate_sum = jnp.dot(full_rows, whole_gate, preferred_element_type=jnp.float32)
    value_sum = jnp.dot(full_rows, whole_value, preferred_element_type=jnp.float32)
    gate_pre = gate_sum.astype(jnp.bfloat16)
    value_pre = value_sum.astype(jnp.bfloat16)
    tail_gate, tail_value, tail_doc = passed_along(
        (
            gate_pre[row_count - rim_rows :],
            value_pre[row_count - rim_rows :],
            doc_ids[row_count - rim_rows :],
        ),
        "sp",
        1,
    )
    ext_gate = jnp.concatenate([tail_gate, gate_pre], 0)
    ext_value = jnp.concatenate([tail_value, value_pre], 0)
    ext_doc = jnp.concatenate([tail_doc, doc_ids], 0)
    gate_mix = jnp.zeros((row_count, local_units), jnp.float32)
    value_mix = jnp.zeros((row_count, local_units), jnp.float32)
    for tap_index in range(CONV):
        valid_tap = (
            (ext_doc[tap_index : tap_index + row_count] == doc_ids)
            & (positions - rim_rows + tap_index >= 0)
        ).astype(jnp.float32)[:, None]
        gate_mix = (
            gate_mix
            + conv_gate[tap_index].astype(jnp.float32)
            * ext_gate[tap_index : tap_index + row_count].astype(jnp.float32)
            * valid_tap
        )
        value_mix = (
            value_mix
            + conv_value[tap_index].astype(jnp.float32)
            * ext_value[tap_index : tap_index + row_count].astype(jnp.float32)
            * valid_tap
        )
    hidden = (value_mix * jax.nn.gelu(gate_mix)).astype(jnp.bfloat16)
    unit_terms = jnp.dot(hidden, whole_down, preferred_element_type=jnp.float32)
    ffn_out = scatter_sum(unit_terms, "tp")
    mixed_two = residual_scale * normed.astype(jnp.float32) + ffn_out
    totals_two = lax.psum((jnp.sum(mixed_two, 1), jnp.sum(mixed_two * mixed_two, 1)), "tp")
    return finish(mixed_two, totals_two, norm2_gain, norm2_bias).astype(jnp.bfloat16)


def solution(mesh):
    placed = (
        P("sp", "tp"),
        P("sp", "tp"),
        P("sp", "tp"),
        P("sp", None),
        P("sp", None),
        P("sp"),
        P(None, "tp"),
        P(None, "tp"),
        P("tp", None),
        P("tp"),
        P("tp"),
        P("sp", "tp"),
        P("sp", "tp"),
        P(None, "tp"),
        P(None, "tp"),
        P("tp", "sp"),
        P("tp"),
        P("tp"),
    )
    return jax.shard_map(
        local, mesh=mesh, in_specs=placed, out_specs=P("sp", "tp"), check_vma=False
    )
```

profile of v0, /device:TPU:0, one launch (start us, length us, event | category | flops | bytes accessed | tf_op | source)
XLA Modules:
  0.0 366.7 jit_solution(3545293043475565079)
XLA Ops:
  6.5 0.7 all-gather.6.cloned.1.call-update
  7.3 0.0 copy-start.7
  7.3 0.0 all-gather.4.cloned.1.call-start
  7.3 0.7 all-gather.4.cloned.1.call-update
  8.0 0.0 all-gather.8.cloned.1.call-start
  8.1 0.8 convert_element_type.115
  8.9 0.3 subtract_convert_fusion.1
  9.2 5.9 %collective-permute-start.6 = (bf16[384,64]{0,1:T(8,128)(2,1)S(1)}, bf16[384,64]{0,1:T(8,128)(2,1)S(1)}, u32[]{:S(2)}, u32[]{:S(2)}) collective-permute-start(bf16[384,64]{0,1:T(8,128)(2,1)S(1)} %pad_maximum_fusion.4), channel_id=1, source_target_pairs={{0,12},{4,16},{8,20},{12,24},{16,28},{1,13},{5,17},{9,21},{13,25},... | collective-permute-start | bytes 147464 | tf_op jit(solution)/shard_map/ppermute | solution.py:21
  15.1 3.5 collective-permute-start.7
  18.6 2.9 collective-permute-start.3
  21.5 1.9 collective-permute-start.4
  23.4 2.8 collective-permute-start.5
  26.2 0.0 all-gather.8.cloned.1.call-update
  26.3 0.2 copy.21
  26.4 0.1 subtract_convert_fusion
  26.6 2.6 collective-permute-start
  29.2 1.3 collective-permute-start.1
  30.5 3.4 collective-permute-start.2
  33.9 1.4 compare_and_fusion
  35.3 11.7 %collective-permute-done = bf16[384,512]{1,0:T(8,128)(2,1)S(1)} collective-permute-done((bf16[384,512]{1,0:T(8,128)(2,1)S(1)}, bf16[384,512]{1,0:T(8,128)(2,1)S(1)}, u32[]{:S(2)}, u32[]{:S(2)}) %collective-permute-start) | collective-permute-done | bytes 393248 | tf_op jit(solution)/shard_map/ppermute | solution.py:21
  47.1 3.3 collective-permute-start.8
  50.4 11.0 %collective-permute-done.1 = bf16[384,512]{1,0:T(8,128)(2,1)S(1)} collective-permute-done((bf16[384,512]{1,0:T(8,128)(2,1)S(1)}, bf16[384,512]{1,0:T(8,128)(2,1)S(1)}, u32[]{:S(2)}, u32[]{:S(2)}) %collective-permute-start.1) | collective-permute-done | bytes 393248 | tf_op jit(solution)/shard_map/ppermute | solution.py:21
  61.6 1.9 convolution_convert_fusion
  63.5 8.3 %fusion.30 = f32[8,1536,384]{2,1,0:T(8,128)} fusion(bf16[1536,8,128]{0,2,1:T(8,128)(2,1)S(1)} %bitcast.56, bf16[384,1024]{1,0:T(8,128)(2,1)S(1)} %copy-done.4), kind=kOutput, calls=%fused_computation.50 | convolution fusion | flops 1207959552 | bytes 22806528 | tf_op jit(solution)/shard_map/qhd,khd->hqk/dot_general | solution.py:118
  71.8 3.5 convolution_convert_fusion.1
  75.3 12.1 %fusion.2 = f32[8,384,1536]{1,2,0:T(8,128)} fusion(f32[8,1536,384]{2,1,0:T(8,128)} %fusion.30, pred[384,1536]{0,1:T(8,128)(4,1)S(1)} %compare_and_fusion, bf16[384,8,32]{0,2,1:T(8,128)(2,1)S(1)} %get-tuple-element.28, bf16[384,8,32]{0,2,1:T(8,128)(2,1)S(1)} %get-tuple-element.27, bf16[384,32]{0,1:T(8,128)(2,1)S(1)} %get-tuple-element.32, ...), kind=kOutput, calls=%fused_computation.3 | convolution fusion | flops 619905024 | bytes 38928384 | tf_op jit(solution)/shard_map/qhr,kr->hqk/dot_general | solution.py:124
  87.4 15.4 %fusion.61 = f32[8,384]{1,0:T(8,128)S(1)} fusion(f32[8,384,1536]{1,2,0:T(8,128)} %fusion.2), kind=kOutput, calls=%fused_computation.129 | output fusion | flops 9438719 | bytes 18886656 | tf_op jit(solution)/shard_map/sub | solution.py:129
  102.8 17.6 %fusion.13 = bf16[8,128,384]{2,1,0:T(8,128)(2,1)S(1)} fusion(bf16[1536,8,128]{0,2,1:T(8,128)(2,1)} %bitcast.57, f32[8,384]{1,0:T(8,128)S(1)} %fusion.61, f32[8,384,1536]{1,2,0:T(8,128)} %fusion.2), kind=kOutput, calls=%fused_computation.28 | convolution fusion | flops 1222513152 | bytes 22818816 | tf_op jit(solution)/shard_map/hqk,khd->qhd/dot_general | solution.py:131
  120.4 4.0 %convolution_convert_fusion.5 = bf16[384,2048]{1,0:T(8,128)(2,1)S(1)} fusion(bf16[384,1024]{0,1:T(8,128)(2,1)S(1)} %bitcast.58, bf16[1024,2048]{1,0:T(8,128)(2,1)} %param.26), kind=kOutput, calls=%fused_computation.15 | convolution fusion | flops 1611399168 | bytes 6553600 | tf_op jit(solution)/shard_map/dot_general | solution.py:138
  124.4 0.1 slice_bitcast_fusion.7
  124.6 1.4 pad_maximum_fusion
  125.9 3.7 %all-to-all-start = ((bf16[4,384,512]{2,1,0:T(8,128)(2,1)}), bf16[4,384,512]{2,1,0:T(8,128)(2,1)S(1)}, u32[]{:S(2)}, u32[]{:S(2)}) async-start(bf16[4,384,512]{2,1,0:T(8,128)(2,1)} %pad_maximum_fusion), calls=%async_computation | async-start | bytes 3145728 | tf_op jit(solution)/shard_map/all_to_all | solution.py:47
  129.7 0.1 slice.108
  129.7 12.4 %collective-permute-start.10 = (s32[2]{0:T(128)S(1)}, s32[2]{0:T(128)S(1)}, u32[]{:S(2)}, u32[]{:S(2)}) collective-permute-start(s32[2]{0:T(128)S(1)} %slice.108), channel_id=1, source_target_pairs={{0,4},{4,8},{8,12},{12,16},{16,20},{20,24},{24,28},{1,5},{5,9},{9,... | collective-permute-start | bytes 32 | tf_op jit(solution)/shard_map/ppermute | solution.py:21
  142.3 0.1 convert_reduce_fusion.4
  142.4 1.1 collective-permute-done.10
  143.5 0.1 pad_add_fusion.1
  143.5 6.1 %all-to-all-done = bf16[4,384,512]{2,1,0:T(8,128)(2,1)S(1)} async-done(((bf16[4,384,512]{2,1,0:T(8,128)(2,1)}), bf16[4,384,512]{2,1,0:T(8,128)(2,1)S(1)}, u32[]{:S(2)}, u32[]{:S(2)}) %all-to-all-start) | async-done | bytes 1572896 | tf_op jit(solution)/shard_map/all_to_all | solution.py:47
  149.7 0.2 convert_reduce_fusion.1
  149.9 0.2 fusion.36
  150.2 6.1 %all-reduce.1 = (f32[384]{0:T(512)S(1)}, f32[384]{0:T(512)S(1)}) all-reduce(f32[384]{0:T(512)S(1)} %get-tuple-element.8, f32[384]{0:T(512)S(1)} %get-tuple-element.7), channel_id=1, replica_groups=mesh['sp'=8,'tp'=4] {'tp'}, use_global_device_ids=true, to_apply=%region_6.7 | all-reduce | flops 768 | bytes 6144 | tf_op jit(solution)/shard_map/psum | solution.py:141
  156.2 0.2 add_convert_fusion.1
  156.5 8.4 %all_gather.15 = bf16[192,2048]{1,0:T(8,128)(2,1)S(1)} all-gather(bf16[192,512]{1,0:T(8,128)(2,1)S(1)} %get-tuple-element.30), channel_id=1, replica_groups=mesh['sp'=8,'tp'=4] {'tp'}, dimensions={1}, use_global_device_ids=true | all-gather | bytes 983040 | tf_op jit(solution)/shard_map/all_gather | solution.py:146
  164.9 0.1 constant_dynamic-update-slice_fusion.5
  165.0 8.7 %all_gather.16 = bf16[192,2048]{1,0:T(8,128)(2,1)S(1)} all-gather(bf16[192,512]{1,0:T(8,128)(2,1)S(1)} %get-tuple-element.29), channel_id=1, replica_groups=mesh['sp'=8,'tp'=4] {'tp'}, dimensions={1}, use_global_device_ids=true | all-gather | bytes 983040 | tf_op jit(solution)/shard_map/all_gather | solution.py:147
  173.7 0.1 constant_dynamic-update-slice_fusion.4
  173.7 0.0 all-gather.6.cloned.1.call-done
  173.7 5.2 %convolution_convert_fusion.3 = bf16[384,1408]{1,0:T(8,128)(2,1)S(1)} fusion(bf16[384,2048]{1,0:T(8,128)(2,1)S(1)} %constant_dynamic-update-slice_fusion.4, bf16[2048,1408]{1,0:T(8,128)(2,1)} %all-gather.6.cloned.1.call-done), kind=kOutput, calls=%fused_computation.13 | convolution fusion | flops 2215133184 | bytes 8421376 | tf_op jit(solution)/shard_map/dot_general | solution.py:151
  179.0 1.0 copy-done.14
  180.0 12.5 %collective-permute-start.11 = (bf16[2,1408]{1,0:T(2,128)(2,1)S(1)}, bf16[2,1408]{1,0:T(2,128)(2,1)S(1)}, u32[]{:S(2)}, u32[]{:S(2)}) collective-permute-start(bf16[2,1408]{1,0:T(2,128)(2,1)S(1)} %slice.137), channel_id=1, source_target_pairs={{0,4},{4,8},{8,12},{12,16},{16,20},{20,24},{24,28},{1,5},{5,9},{9,... | collective-permute-start | bytes 16904 | tf_op jit(solution)/shard_map/ppermute | solution.py:21
  192.5 30.3 %all-gather.4.cloned.1.call-done = bf16[2048,1408]{1,0:T(8,128)(2,1)} async-done(((bf16[256,1408]{1,0:T(8,128)(2,1)}), bf16[2048,1408]{1,0:T(8,128)(2,1)}) %all-gather.4.cloned.1.call-update) | async-done | bytes 5767184 | tf_op jit(solution)/shard_map/all_gather | solution.py:85
  222.8 5.2 %convolution_convert_fusion.4 = bf16[384,1408]{1,0:T(8,128)(2,1)S(1)} fusion(bf16[384,2048]{1,0:T(8,128)(2,1)S(1)} %constant_dynamic-update-slice_fusion.4, bf16[2048,1408]{1,0:T(8,128)(2,1)} %all-gather.4.cloned.1.call-done), kind=kOutput, calls=%fused_computation.14 | convolution fusion | flops 2215133184 | bytes 8421376 | tf_op jit(solution)/shard_map/dot_general | solution.py:152
  228.1 2.5 collective-permute-start.9
  230.6 0.1 fusion.49
  230.7 85.7 %all-gather.8.cloned.1.call-done = bf16[1408,2048]{1,0:T(8,128)(2,1)} async-done(((bf16[1408,256]{1,0:T(8,128)(2,1)}), bf16[1408,2048]{1,0:T(8,128)(2,1)}) %all-gather.8.cloned.1.call-update) | async-done | bytes 5767184 | tf_op jit(solution)/shard_map/all_gather | solution.py:86
  316.4 9.3 %convolution_convert_fusion.2 = bf16[384,2048]{1,0:T(8,128)(2,1)S(1)} fusion(bf16[1408,2048]{1,0:T(8,128)(2,1)} %all-gather.8.cloned.1.call-done, bf16[384,1408]{1,0:T(8,128)(2,1)} %copy-done.14, bf16[384,1408]{1,0:T(8,128)(2,1)} %copy-done.15, bf16[2,1408]{1,0:T(2,128)(2,1)S(1)} %collective-permute-done.11, ...), kind=kOutput, calls=%fused_computation.12 | convolution fusion | flops 2239168512 | bytes 9552384 | tf_op jit(solution)/shard_map/dot_general | solution.py:187
  325.7 0.1 slice_bitcast_fusion.3
  325.8 1.4 pad_maximum_fusion.1
  327.2 3.7 %all-to-all-start.1 = ((bf16[4,384,512]{2,1,0:T(8,128)(2,1)}), bf16[4,384,512]{2,1,0:T(8,128)(2,1)S(1)}, u32[]{:S(2)}, u32[]{:S(2)}) async-start(bf16[4,384,512]{2,1,0:T(8,128)(2,1)} %pad_maximum_fusion.1), calls=%async_computation.1 | async-start | bytes 3145728 | tf_op jit(solution)/shard_map/all_to_all | solution.py:47
  331.0 20.0 %all-to-all-done.1 = bf16[4,384,512]{2,1,0:T(8,128)(2,1)S(1)} async-done(((bf16[4,384,512]{2,1,0:T(8,128)(2,1)}), bf16[4,384,512]{2,1,0:T(8,128)(2,1)S(1)}, u32[]{:S(2)}, u32[]{:S(2)}) %all-to-all-start.1) | async-done | bytes 1572896 | tf_op jit(solution)/shard_map/all_to_all | solution.py:47
  350.9 0.2 convert_reduce_fusion
  351.2 1.2 fusion.37
  352.4 5.8 %all-reduce = (f32[384]{0:T(512)S(1)}, f32[384]{0:T(512)S(1)}) all-reduce(f32[384]{0:T(512)S(1)} %get-tuple-element.6, f32[384]{0:T(512)S(1)} %get-tuple-element.5), channel_id=1, replica_groups=mesh['sp'=8,'tp'=4] {'tp'}, use_global_device_ids=true, to_apply=%region_11.12 | all-reduce | flops 768 | bytes 6144 | tf_op jit(solution)/shard_map/psum | solution.py:190
  358.2 2.0 add_convert_fusion
  (63 shorter events, 0.3 us)
Async XLA Ops:
  6.5 55.0 %copy-start = (bf16[512,1024]{1,0:T(8,128)(2,1)S(1)}, bf16[512,1024]{1,0:T(8,128)(2,1)}, u32[]{:S(2)}) copy-start(bf16[512,1024]{1,0:T(8,128)(2,1)} %param.24) | copy-start | bytes 3145732
  6.5 19.7 %copy-start.6 = (bf16[384,512]{1,0:T(8,128)(2,1)S(1)}, bf16[384,512]{1,0:T(8,128)(2,1)}, u32[]{:S(2)}) copy-start(bf16[384,512]{1,0:T(8,128)(2,1)} %param.20) | copy-start | bytes 1179652
  6.5 167.2 %all-gather.6.cloned.1.call-start = ((), (), s32[]{:S(2)}) async-start(), calls=%async_computation.3 | async-start | bytes 6488064 | tf_op jit(solution)/shard_map/all_gather | solution.py:84
  7.3 19.3 %copy-start.5 = (bf16[384,512]{1,0:T(8,128)(2,1)S(1)}, bf16[384,512]{1,0:T(8,128)(2,1)}, u32[]{:S(2)}) copy-start(bf16[384,512]{1,0:T(8,128)(2,1)} %param.21) | copy-start | bytes 1179652
  7.3 26.6 %copy-start.7 = (s32[384]{0:T(512)S(1)}, s32[384]{0:T(512)}, u32[]{:S(2)}) copy-start(s32[384]{0:T(512)} %param.23) | copy-start | bytes 4612
  7.3 215.5 %all-gather.4.cloned.1.call-start = ((), (), s32[]{:S(2)}) async-start(), calls=%async_computation.2 | async-start | bytes 6488064 | tf_op jit(solution)/shard_map/all_gather | solution.py:85
  8.0 308.3 %all-gather.8.cloned.1.call-start = ((), (), s32[]{:S(2)}) async-start(), calls=%async_computation.4 | async-start | bytes 6488064 | tf_op jit(solution)/shard_map/all_gather | solution.py:86
  9.2 66.1 %collective-permute-start.6 = (bf16[384,64]{0,1:T(8,128)(2,1)S(1)}, bf16[384,64]{0,1:T(8,128)(2,1)S(1)}, u32[]{:S(2)}, u32[]{:S(2)}) collective-permute-start(bf16[384,64]{0,1:T(8,128)(2,1)S(1)} %pad_maximum_fusion.4), channel_id=1, source_target_pairs={{0,12},{4,16},{8,20},{12,24},{16,28},{1,13},{5,17},{9,21},{13,25},... | collective-permute-start | bytes 147464 | tf_op jit(solution)/shard_map/ppermute | solution.py:21
  15.1 60.2 %collective-permute-start.7 = (bf16[384,64]{0,1:T(8,128)(2,1)S(1)}, bf16[384,64]{0,1:T(8,128)(2,1)S(1)}, u32[]{:S(2)}, u32[]{:S(2)}) collective-permute-start(bf16[384,64]{0,1:T(8,128)(2,1)S(1)} %pad_maximum_fusion.4), channel_id=1, source_target_pairs={{0,8},{4,12},{8,16},{12,20},{16,24},{20,28},{1,9},{5,13},{9,17},{1... | collective-permute-start | bytes 147464 | tf_op jit(solution)/shard_map/ppermute | solution.py:21
  18.6 8.0 %collective-permute-start.3 = (s32[384]{0:T(512)}, s32[384]{0:T(512)S(1)}, u32[]{:S(2)}, u32[]{:S(2)}) collective-permute-start(s32[384]{0:T(512)} %param.23), channel_id=1, source_target_pairs={{0,12},{4,16},{8,20},{12,24},{16,28},{1,13},{5,17},{9,21},{13,25},... | collective-permute-start | bytes 4616 | tf_op jit(solution)/shard_map/ppermute | solution.py:21
  21.5 7.7 %collective-permute-start.4 = (s32[384]{0:T(512)}, s32[384]{0:T(512)S(1)}, u32[]{:S(2)}, u32[]{:S(2)}) collective-permute-start(s32[384]{0:T(512)} %param.23), channel_id=1, source_target_pairs={{0,8},{4,12},{8,16},{12,20},{16,24},{20,28},{1,9},{5,13},{9,17},{1... | collective-permute-start | bytes 4616 | tf_op jit(solution)/shard_map/ppermute | solution.py:21
  23.4 7.1 %collective-permute-start.5 = (s32[384]{0:T(512)}, s32[384]{0:T(512)S(1)}, u32[]{:S(2)}, u32[]{:S(2)}) collective-permute-start(s32[384]{0:T(512)} %param.23), channel_id=1, source_target_pairs={{0,4},{4,8},{8,12},{12,16},{16,20},{20,24},{24,28},{1,5},{5,9},{9,... | collective-permute-start | bytes 4616 | tf_op jit(solution)/shard_map/ppermute | solution.py:21
  26.6 20.5 %collective-permute-start = (bf16[384,512]{1,0:T(8,128)(2,1)S(1)}, bf16[384,512]{1,0:T(8,128)(2,1)S(1)}, u32[]{:S(2)}, u32[]{:S(2)}) collective-permute-start(bf16[384,512]{1,0:T(8,128)(2,1)S(1)} %copy-done.5), channel_id=1, source_target_pairs={{0,12},{4,16},{8,20},{12,24},{16,28},{1,13},{5,17},{9,21},{13,25},... | collective-permute-start | bytes 1179656 | tf_op jit(solution)/shard_map/ppermute | solution.py:21
  29.2 32.3 %collective-permute-start.1 = (bf16[384,512]{1,0:T(8,128)(2,1)S(1)}, bf16[384,512]{1,0:T(8,128)(2,1)S(1)}, u32[]{:S(2)}, u32[]{:S(2)}) collective-permute-start(bf16[384,512]{1,0:T(8,128)(2,1)S(1)} %copy-done.5), channel_id=1, source_target_pairs={{0,8},{4,12},{8,16},{12,20},{16,24},{20,28},{1,9},{5,13},{9,17},{1... | collective-permute-start | bytes 1179656 | tf_op jit(solution)/shard_map/ppermute | solution.py:21
  30.5 31.0 %collective-permute-start.2 = (bf16[384,512]{1,0:T(8,128)(2,1)S(1)}, bf16[384,512]{1,0:T(8,128)(2,1)S(1)}, u32[]{:S(2)}, u32[]{:S(2)}) collective-permute-start(bf16[384,512]{1,0:T(8,128)(2,1)S(1)} %copy-done.5), channel_id=1, source_target_pairs={{0,4},{4,8},{8,12},{12,16},{16,20},{20,24},{24,28},{1,5},{5,9},{9,... | collective-permute-start | bytes 1179656 | tf_op jit(solution)/shard_map/ppermute | solution.py:21
  47.1 28.3 %collective-permute-start.8 = (bf16[384,64]{0,1:T(8,128)(2,1)S(1)}, bf16[384,64]{0,1:T(8,128)(2,1)S(1)}, u32[]{:S(2)}, u32[]{:S(2)}) collective-permute-start(bf16[384,64]{0,1:T(8,128)(2,1)S(1)} %pad_maximum_fusion.4), channel_id=1, source_target_pairs={{0,4},{4,8},{8,12},{12,16},{16,20},{20,24},{24,28},{1,5},{5,9},{9,... | collective-permute-start | bytes 147464 | tf_op jit(solution)/shard_map/ppermute | solution.py:21
  61.6 1.9 copy-start.4
  63.5 8.3 %copy-start.16 = (bf16[512,1024]{1,0:T(8,128)(2,1)S(1)}, bf16[512,1024]{1,0:T(8,128)(2,1)}, u32[]{:S(2)}) copy-start(bf16[512,1024]{1,0:T(8,128)(2,1)} %param.25) | copy-start | bytes 3145732
  125.9 16.3 %copy-start.10 = (bf16[512]{0:T(512)(128)(2,1)S(1)}, bf16[512]{0:T(512)(128)(2,1)}, u32[]{:S(2)}) copy-start(bf16[512]{0:T(512)(128)(2,1)} %param.27) | copy-start | bytes 3076
  125.9 16.3 %copy-start.11 = (bf16[512]{0:T(512)(128)(2,1)S(1)}, bf16[512]{0:T(512)(128)(2,1)}, u32[]{:S(2)}) copy-start(bf16[512]{0:T(512)(128)(2,1)} %param.28) | copy-start | bytes 3076
  125.9 16.3 %copy-start.8 = (bf16[3,1408]{1,0:T(4,128)(2,1)S(1)}, bf16[3,1408]{1,0:T(4,128)(2,1)}, u32[]{:S(2)}) copy-start(bf16[3,1408]{1,0:T(4,128)(2,1)} %param.31) | copy-start | bytes 25348
  125.9 16.3 %copy-start.9 = (bf16[3,1408]{1,0:T(4,128)(2,1)S(1)}, bf16[3,1408]{1,0:T(4,128)(2,1)}, u32[]{:S(2)}) copy-start(bf16[3,1408]{1,0:T(4,128)(2,1)} %param.32) | copy-start | bytes 25348
  125.9 24.0 %copy-start.3 = (bf16[384,512]{1,0:T(8,128)(2,1)S(1)}, bf16[384,512]{1,0:T(8,128)(2,1)}, u32[]{:S(2)}) copy-start(bf16[384,512]{1,0:T(8,128)(2,1)} %param.18) | copy-start | bytes 1179652
  125.9 23.7 %all-to-all-start = ((bf16[4,384,512]{2,1,0:T(8,128)(2,1)}), bf16[4,384,512]{2,1,0:T(8,128)(2,1)S(1)}, u32[]{:S(2)}, u32[]{:S(2)}) async-start(bf16[4,384,512]{2,1,0:T(8,128)(2,1)} %pad_maximum_fusion), calls=%async_computation | async-start | bytes 3145728 | tf_op jit(solution)/shard_map/all_to_all | solution.py:47
  129.7 13.7 %collective-permute-start.10 = (s32[2]{0:T(128)S(1)}, s32[2]{0:T(128)S(1)}, u32[]{:S(2)}, u32[]{:S(2)}) collective-permute-start(s32[2]{0:T(128)S(1)} %slice.108), channel_id=1, source_target_pairs={{0,4},{4,8},{8,12},{12,16},{16,20},{20,24},{24,28},{1,5},{5,9},{9,... | collective-permute-start | bytes 32 | tf_op jit(solution)/shard_map/ppermute | solution.py:21
  156.5 17.2 %copy-start.2 = (bf16[384,512]{1,0:T(8,128)(2,1)}, bf16[384,512]{1,0:T(8,128)(2,1)S(1)}, u32[]{:S(2)}) copy-start(bf16[384,512]{1,0:T(8,128)(2,1)S(1)} %add_convert_fusion.1) | copy-start | bytes 1179652
  179.0 1.0 copy-start.14
  180.0 136.4 %collective-permute-start.11 = (bf16[2,1408]{1,0:T(2,128)(2,1)S(1)}, bf16[2,1408]{1,0:T(2,128)(2,1)S(1)}, u32[]{:S(2)}, u32[]{:S(2)}) collective-permute-start(bf16[2,1408]{1,0:T(2,128)(2,1)S(1)} %slice.137), channel_id=1, source_target_pairs={{0,4},{4,8},{8,12},{12,16},{16,20},{20,24},{24,28},{1,5},{5,9},{9,... | collective-permute-start | bytes 16904 | tf_op jit(solution)/shard_map/ppermute | solution.py:21
  228.0 2.5 copy-start.15
  228.1 88.3 %collective-permute-start.9 = (bf16[2,1408]{1,0:T(2,128)(2,1)S(1)}, bf16[2,1408]{1,0:T(2,128)(2,1)S(1)}, u32[]{:S(2)}, u32[]{:S(2)}) collective-permute-start(bf16[2,1408]{1,0:T(2,128)(2,1)S(1)} %slice.134), channel_id=1, source_target_pairs={{0,4},{4,8},{8,12},{12,16},{16,20},{20,24},{24,28},{1,5},{5,9},{9,... | collective-permute-start | bytes 16904 | tf_op jit(solution)/shard_map/ppermute | solution.py:21
  327.2 3.7 %copy-start.12 = (bf16[512]{0:T(512)(128)(2,1)S(1)}, bf16[512]{0:T(512)(128)(2,1)}, u32[]{:S(2)}) copy-start(bf16[512]{0:T(512)(128)(2,1)} %param.34) | copy-start | bytes 3076
  327.2 3.7 %copy-start.13 = (bf16[512]{0:T(512)(128)(2,1)S(1)}, bf16[512]{0:T(512)(128)(2,1)}, u32[]{:S(2)}) copy-start(bf16[512]{0:T(512)(128)(2,1)} %param.35) | copy-start | bytes 3076
  327.2 23.7 %all-to-all-start.1 = ((bf16[4,384,512]{2,1,0:T(8,128)(2,1)}), bf16[4,384,512]{2,1,0:T(8,128)(2,1)S(1)}, u32[]{:S(2)}, u32[]{:S(2)}) async-start(bf16[4,384,512]{2,1,0:T(8,128)(2,1)} %pad_maximum_fusion.1), calls=%async_computation.1 | async-start | bytes 3145728 | tf_op jit(solution)/shard_map/all_to_all | solution.py:47
  330.9 29.2 %copy-start.1 = (bf16[512,1024]{1,0:T(8,128)(2,1)S(1)}, bf16[512,1024]{1,0:T(8,128)(2,1)}, u32[]{:S(2)}) copy-start(bf16[512,1024]{1,0:T(8,128)(2,1)} %param.24) | copy-start | bytes 3145732
Sparse Core Ops, SparseCore 0:
  9.5 118.1 all-gather.5
  129.9 92.8 all-gather.3
  224.8 91.4 all-gather.7
where the time goes:
time: 368 us; the launch traced here: 367 us
  waiting for transfers between devices  167 us (45%)
  matrix products  67.2 us (18%)
  starting transfers between devices  62.4 us (17%)
  blocking collectives  28.9 us (8%)
  other arithmetic  25.2 us (7%)
  between operations  13.7 us (4%)
    all_gather x1, waiting for transfers between devices, local(): lax.all_gather(ffn_down, 'sp', axis=1, tiled=True)  85.7 us
    ppermute x12, starting transfers between devices, passed_along(): return lax.ppermute(value, axis, pairs)  55 us
    all_gather x1, waiting for transfers between devices, local(): lax.all_gather(ffn_value, 'sp', axis=0, tiled=True)  30.3 us
    all_to_all x2, waiting for transfers between devices, scatter_sum(): got = lax.all_to_all(parts.astype(jnp.bfloat16), axis, 0, 0)  26.1 us
    ppermute x12, waiting for transfers between devices, passed_along(): return lax.ppermute(value, axis, pairs)  23.9 us
    dot_general x1, matrix products, local(): jnp.einsum('hqk,khd->qhd', weights, values.reshape(window, head_count, VD...  17.6 us
    sub x1, other arithmetic, local(): weights = jnp.exp(scores - row_max)  15.4 us
    dot_general x1, matrix products, local(): jnp.einsum('qhr,kr->hqk', turned_query, win_key, preferred_element_type=j...  12.1 us
  transfers between devices with their start and end apart: 17, of which 7 were waited for; matrix products, arithmetic and copies ran while one was open for 22% of the time, Pallas kernels for 0%

commit v1 on v0

--- a/solution.py
+++ b/solution.py
@@ -83,7 +83,7 @@
     whole_gate, whole_value, whole_down = (
         lax.all_gather(ffn_gate, "sp", axis=0, tiled=True),
         lax.all_gather(ffn_value, "sp", axis=0, tiled=True),
-        lax.all_gather(ffn_down, "sp", axis=1, tiled=True),
+        jnp.concatenate(jax.lax.all_gather(ffn_down, "sp"), axis=1),
     )
     offset = lax.axis_index("sp") * row_count
     positions = offset + jnp.arange(row_count, dtype=jnp.int32)

time: 368 us -> 375 us (1.019)
  local copies, waits for them, and re-layouts: 1.76 us -> 10.1 us
    reshape x0 -> x1, local copies, waits for them, and re-layouts: none -> 8.34 us  [local(): jnp.concatenate(jax.lax.all_gather(ffn_down, 'sp'), axis=1)]
  transfers between devices with their start and end apart: 17 -> 17, of which waited for: 7 -> 7; matrix products, arithmetic and copies ran while one was open for 22% -> 23% of each run, Pallas kernels for 0% -> 0%
where the time goes in v1:
time: 375 us; the launch traced here: 374 us
  waiting for transfers between devices  167 us (45%)
  matrix products  67.3 us (18%)
  starting transfers between devices  62.4 us (17%)
  blocking collectives  28.9 us (8%)
  other arithmetic  25.1 us (7%)
  between operations  13.7 us (4%)
  local copies, waits for them, and re-layouts  10.1 us (3%)
    all_gather x1, waiting for transfers between devices, local(): jax.lax.all_gather(ffn_down, 'sp')  85 us
    ppermute x12, starting transfers between devices, passed_along(): return lax.ppermute(value, axis, pairs)  54.9 us
    all_gather x1, waiting for transfers between devices, local(): lax.all_gather(ffn_value, 'sp', axis=0, tiled=True)  30.4 us
    all_to_all x2, waiting for transfers between devices, scatter_sum(): got = lax.all_to_all(parts.astype(jnp.bfloat16), axis, 0, 0)  26.1 us
    ppermute x12, waiting for transfers between devices, passed_along(): return lax.ppermute(value, axis, pairs)  23.9 us
    dot_general x1, matrix products, local(): jnp.einsum('hqk,khd->qhd', weights, values.reshape(window, head_count, VD...  17.6 us
    sub x1, other arithmetic, local(): weights = jnp.exp(scores - row_max)  15.3 us
    dot_general x1, matrix products, local(): jnp.einsum('qhr,kr->hqk', turned_query, win_key, preferred_element_type=j...  12.1 us
  transfers between devices with their start and end apart: 17, of which 7 were waited for; matrix products, arithmetic and copies ran while one was open for 23% of the time, Pallas kernels for 0%

profile of v1, /device:TPU:0, one launch (start us, length us, event | category | flops | bytes accessed | tf_op | source)
XLA Modules:
  0.0 374.5 jit_solution(16778433980352434974)
XLA Ops:
  6.5 0.7 all-gather.7.cloned.1.call-update
  7.3 0.0 all-gather.5.cloned.1.call-start
  7.3 0.7 all-gather.5.cloned.1.call-update
  8.0 0.0 all-gather.9.cloned.1.call-start
  8.1 0.8 convert_element_type.115
  8.9 0.3 subtract_convert_fusion.1
  9.2 5.9 %collective-permute-start.6 = (bf16[384,64]{0,1:T(8,128)(2,1)S(1)}, bf16[384,64]{0,1:T(8,128)(2,1)S(1)}, u32[]{:S(2)}, u32[]{:S(2)}) collective-permute-start(bf16[384,64]{0,1:T(8,128)(2,1)S(1)} %pad_maximum_fusion.4), channel_id=1, source_target_pairs={{0,12},{4,16},{8,20},{12,24},{16,28},{1,13},{5,17},{9,21},{13,25},... | collective-permute-start | bytes 147464 | tf_op jit(solution)/shard_map/ppermute | solution.py:21
  15.1 3.5 collective-permute-start.7
  18.6 2.9 collective-permute-start.3
  21.5 1.9 collective-permute-start.4
  23.4 2.8 collective-permute-start.5
  26.2 0.0 all-gather.9.cloned.1.call-update
  26.3 0.2 copy.29
  26.4 0.1 subtract_convert_fusion
  26.6 2.6 collective-permute-start
  29.2 1.3 collective-permute-start.1
  30.5 3.4 collective-permute-start.2
  33.9 1.4 compare_and_fusion
  35.3 11.7 %collective-permute-done = bf16[384,512]{1,0:T(8,128)(2,1)S(1)} collective-permute-done((bf16[384,512]{1,0:T(8,128)(2,1)S(1)}, bf16[384,512]{1,0:T(8,128)(2,1)S(1)}, u32[]{:S(2)}, u32[]{:S(2)}) %collective-permute-start) | collective-permute-done | bytes 393248 | tf_op jit(solution)/shard_map/ppermute | solution.py:21
  47.1 3.3 collective-permute-start.8
  50.4 11.0 %collective-permute-done.1 = bf16[384,512]{1,0:T(8,128)(2,1)S(1)} collective-permute-done((bf16[384,512]{1,0:T(8,128)(2,1)S(1)}, bf16[384,512]{1,0:T(8,128)(2,1)S(1)}, u32[]{:S(2)}, u32[]{:S(2)}) %collective-permute-start.1) | collective-permute-done | bytes 393248 | tf_op jit(solution)/shard_map/ppermute | solution.py:21
  61.6 1.9 convolution_convert_fusion
  63.5 8.3 %fusion.30 = f32[8,1536,384]{2,1,0:T(8,128)} fusion(bf16[1536,8,128]{0,2,1:T(8,128)(2,1)S(1)} %bitcast.62, bf16[384,1024]{1,0:T(8,128)(2,1)S(1)} %copy-done.4), kind=kOutput, calls=%fused_computation.50 | convolution fusion | flops 1207959552 | bytes 22806528 | tf_op jit(solution)/shard_map/qhd,khd->hqk/dot_general | solution.py:118
  71.8 3.5 convolution_convert_fusion.1
  75.3 12.1 %fusion.2 = f32[8,384,1536]{1,2,0:T(8,128)} fusion(f32[8,1536,384]{2,1,0:T(8,128)} %fusion.30, pred[384,1536]{0,1:T(8,128)(4,1)S(1)} %compare_and_fusion, bf16[384,8,32]{0,2,1:T(8,128)(2,1)S(1)} %get-tuple-element.28, bf16[384,8,32]{0,2,1:T(8,128)(2,1)S(1)} %get-tuple-element.27, bf16[384,32]{0,1:T(8,128)(2,1)S(1)} %get-tuple-element.32, ...), kind=kOutput, calls=%fused_computation.3 | convolution fusion | flops 619905024 | bytes 38928384 | tf_op jit(solution)/shard_map/qhr,kr->hqk/dot_general | solution.py:124
  87.4 15.3 %fusion.61 = f32[8,384]{1,0:T(8,128)S(1)} fusion(f32[8,384,1536]{1,2,0:T(8,128)} %fusion.2), kind=kOutput, calls=%fused_computation.129 | output fusion | flops 9438719 | bytes 18886656 | tf_op jit(solution)/shard_map/sub | solution.py:129
  102.8 17.6 %fusion.13 = bf16[8,128,384]{2,1,0:T(8,128)(2,1)S(1)} fusion(bf16[1536,8,128]{0,2,1:T(8,128)(2,1)} %bitcast.63, f32[8,384]{1,0:T(8,128)S(1)} %fusion.61, f32[8,384,1536]{1,2,0:T(8,128)} %fusion.2), kind=kOutput, calls=%fused_computation.28 | convolution fusion | flops 1222513152 | bytes 22818816 | tf_op jit(solution)/shard_map/hqk,khd->qhd/dot_general | solution.py:131
  120.4 4.0 %convolution_convert_fusion.5 = bf16[384,2048]{1,0:T(8,128)(2,1)S(1)} fusion(bf16[384,1024]{0,1:T(8,128)(2,1)S(1)} %bitcast.64, bf16[1024,2048]{1,0:T(8,128)(2,1)} %param.26), kind=kOutput, calls=%fused_computation.15 | convolution fusion | flops 1611399168 | bytes 6553600 | tf_op jit(solution)/shard_map/dot_general | solution.py:138
  124.4 0.1 slice_bitcast_fusion.7
  124.5 1.4 pad_maximum_fusion
  125.9 3.7 all-to-all-start
  129.6 0.1 slice.108
  129.7 12.4 %collective-permute-start.10 = (s32[2]{0:T(128)S(1)}, s32[2]{0:T(128)S(1)}, u32[]{:S(2)}, u32[]{:S(2)}) collective-permute-start(s32[2]{0:T(128)S(1)} %slice.108), channel_id=1, source_target_pairs={{0,4},{4,8},{8,12},{12,16},{16,20},{20,24},{24,28},{1,5},{5,9},{9,... | collective-permute-start | bytes 32 | tf_op jit(solution)/shard_map/ppermute | solution.py:21
  142.2 0.1 convert_reduce_fusion.4
  142.3 1.1 collective-permute-done.10
  143.4 0.1 pad_add_fusion.1
  143.5 6.1 %all-to-all-done = bf16[4,384,512]{2,1,0:T(8,128)(2,1)S(1)} async-done(((bf16[4,384,512]{2,1,0:T(8,128)(2,1)}), bf16[4,384,512]{2,1,0:T(8,128)(2,1)S(1)}, u32[]{:S(2)}, u32[]{:S(2)}) %all-to-all-start) | async-done | bytes 1572896 | tf_op jit(solution)/shard_map/all_to_all | solution.py:47
  149.6 0.2 convert_reduce_fusion.1
  149.9 0.2 fusion.36
  150.1 6.1 %all-reduce.1 = (f32[384]{0:T(512)S(1)}, f32[384]{0:T(512)S(1)}) all-reduce(f32[384]{0:T(512)S(1)} %get-tuple-element.8, f32[384]{0:T(512)S(1)} %get-tuple-element.7), channel_id=1, replica_groups=mesh['sp'=8,'tp'=4] {'tp'}, use_global_device_ids=true, to_apply=%region_6.7 | all-reduce | flops 768 | bytes 6144 | tf_op jit(solution)/shard_map/psum | solution.py:141
  156.2 0.2 add_convert_fusion.1
  156.5 8.4 %all_gather.18 = bf16[192,2048]{1,0:T(8,128)(2,1)S(1)} all-gather(bf16[192,512]{1,0:T(8,128)(2,1)S(1)} %get-tuple-element.30), channel_id=1, replica_groups=mesh['sp'=8,'tp'=4] {'tp'}, dimensions={1}, use_global_device_ids=true | all-gather | bytes 983040 | tf_op jit(solution)/shard_map/all_gather | solution.py:146
  164.8 0.1 constant_dynamic-update-slice_fusion.5
  164.9 8.7 %all_gather.19 = bf16[192,2048]{1,0:T(8,128)(2,1)S(1)} all-gather(bf16[192,512]{1,0:T(8,128)(2,1)S(1)} %get-tuple-element.29), channel_id=1, replica_groups=mesh['sp'=8,'tp'=4] {'tp'}, dimensions={1}, use_global_device_ids=true | all-gather | bytes 983040 | tf_op jit(solution)/shard_map/all_gather | solution.py:147
  173.6 0.1 constant_dynamic-update-slice_fusion.4
  173.7 0.0 all-gather.7.cloned.1.call-done
  173.7 5.2 %convolution_convert_fusion.3 = bf16[384,1408]{1,0:T(8,128)(2,1)S(1)} fusion(bf16[384,2048]{1,0:T(8,128)(2,1)S(1)} %constant_dynamic-update-slice_fusion.4, bf16[2048,1408]{1,0:T(8,128)(2,1)} %all-gather.7.cloned.1.call-done), kind=kOutput, calls=%fused_computation.13 | convolution fusion | flops 2215133184 | bytes 8421376 | tf_op jit(solution)/shard_map/dot_general | solution.py:151
  178.9 1.0 copy-done.14
  180.0 12.5 %collective-permute-start.11 = (bf16[2,1408]{1,0:T(2,128)(2,1)S(1)}, bf16[2,1408]{1,0:T(2,128)(2,1)S(1)}, u32[]{:S(2)}, u32[]{:S(2)}) collective-permute-start(bf16[2,1408]{1,0:T(2,128)(2,1)S(1)} %slice.137), channel_id=1, source_target_pairs={{0,4},{4,8},{8,12},{12,16},{16,20},{20,24},{24,28},{1,5},{5,9},{9,... | collective-permute-start | bytes 16904 | tf_op jit(solution)/shard_map/ppermute | solution.py:21
  192.4 30.4 %all-gather.5.cloned.1.call-done = bf16[2048,1408]{1,0:T(8,128)(2,1)} async-done(((bf16[256,1408]{1,0:T(8,128)(2,1)}), bf16[2048,1408]{1,0:T(8,128)(2,1)}) %all-gather.5.cloned.1.call-update) | async-done | bytes 5767184 | tf_op jit(solution)/shard_map/all_gather | solution.py:85
  222.8 5.2 %convolution_convert_fusion.4 = bf16[384,1408]{1,0:T(8,128)(2,1)S(1)} fusion(bf16[384,2048]{1,0:T(8,128)(2,1)S(1)} %constant_dynamic-update-slice_fusion.4, bf16[2048,1408]{1,0:T(8,128)(2,1)} %all-gather.5.cloned.1.call-done), kind=kOutput, calls=%fused_computation.14 | convolution fusion | flops 2215133184 | bytes 8421376 | tf_op jit(solution)/shard_map/dot_general | solution.py:152
  228.1 2.5 collective-permute-start.9
  230.6 0.1 fusion.49
  230.7 85.0 %all-gather.9.cloned.1.call-done = bf16[11264,256]{1,0:T(8,128)(2,1)} async-done(((bf16[1408,256]{1,0:T(8,128)(2,1)}), bf16[11264,256]{1,0:T(8,128)(2,1)}) %all-gather.9.cloned.1.call-update) | async-done | bytes 5767184 | tf_op jit(solution)/shard_map/all_gather | solution.py:86
  315.7 8.3 %copy.31 = bf16[1408,8,256]{0,2,1:T(8,128)(2,1)} copy(bf16[1408,8,256]{2,0,1:T(8,128)(2,1)} %bitcast.59) | data formatting | bytes 11534336 | tf_op jit(solution)/shard_map/reshape | solution.py:86
  324.0 9.5 %convolution_convert_fusion.2 = bf16[384,2048]{1,0:T(8,128)(2,1)S(1)} fusion(bf16[1408,2048]{0,1:T(8,128)(2,1)} %bitcast.60, bf16[384,1408]{1,0:T(8,128)(2,1)S(1)} %copy-done.15, bf16[384,1408]{1,0:T(8,128)(2,1)} %copy-done.16, bf16[2,1408]{1,0:T(2,128)(2,1)S(1)} %collective-permute-done.11, bf16[2,1408]{1,0:T(2,128)(2,1)S(1)} %collective-permute-done.9, ...), kind=kOutput, calls=%fused_computation.12 | convolution fusion | flops 2239168512 | bytes 9552384 | tf_op jit(solution)/shard_map/dot_general | solution.py:187
  333.5 0.1 slice_bitcast_fusion.3
  333.6 1.4 pad_maximum_fusion.1
  335.0 3.7 all-to-all-start.1
  338.7 20.0 %all-to-all-done.1 = bf16[4,384,512]{2,1,0:T(8,128)(2,1)S(1)} async-done(((bf16[4,384,512]{2,1,0:T(8,128)(2,1)}), bf16[4,384,512]{2,1,0:T(8,128)(2,1)S(1)}, u32[]{:S(2)}, u32[]{:S(2)}) %all-to-all-start.1) | async-done | bytes 1572896 | tf_op jit(solution)/shard_map/all_to_all | solution.py:47
  358.7 0.2 convert_reduce_fusion
  358.9 1.2 fusion.37
  360.2 5.8 %all-reduce = (f32[384]{0:T(512)S(1)}, f32[384]{0:T(512)S(1)}) all-reduce(f32[384]{0:T(512)S(1)} %get-tuple-element.6, f32[384]{0:T(512)S(1)} %get-tuple-element.5), channel_id=1, replica_groups=mesh['sp'=8,'tp'=4] {'tp'}, use_global_device_ids=true, to_apply=%region_11.12 | all-reduce | flops 768 | bytes 6144 | tf_op jit(solution)/shard_map/psum | solution.py:190
  366.0 2.0 add_convert_fusion
  (66 shorter events, 0.4 us)
Async XLA Ops:
  6.5 55.0 %copy-start = (bf16[512,1024]{1,0:T(8,128)(2,1)S(1)}, bf16[512,1024]{1,0:T(8,128)(2,1)}, u32[]{:S(2)}) copy-start(bf16[512,1024]{1,0:T(8,128)(2,1)} %param.24) | copy-start | bytes 3145732
  6.5 19.7 %copy-start.6 = (bf16[384,512]{1,0:T(8,128)(2,1)S(1)}, bf16[384,512]{1,0:T(8,128)(2,1)}, u32[]{:S(2)}) copy-start(bf16[384,512]{1,0:T(8,128)(2,1)} %param.20) | copy-start | bytes 1179652
  6.5 167.1 %all-gather.7.cloned.1.call-start = ((), (), s32[]{:S(2)}) async-start(), calls=%async_computation.3 | async-start | bytes 6488064 | tf_op jit(solution)/shard_map/all_gather | solution.py:84
  7.3 19.3 %copy-start.5 = (bf16[384,512]{1,0:T(8,128)(2,1)S(1)}, bf16[384,512]{1,0:T(8,128)(2,1)}, u32[]{:S(2)}) copy-start(bf16[384,512]{1,0:T(8,128)(2,1)} %param.21) | copy-start | bytes 1179652
  7.3 26.6 %copy-start.7 = (s32[384]{0:T(512)S(1)}, s32[384]{0:T(512)}, u32[]{:S(2)}) copy-start(s32[384]{0:T(512)} %param.23) | copy-start | bytes 4612
  7.3 215.5 %all-gather.5.cloned.1.call-start = ((), (), s32[]{:S(2)}) async-start(), calls=%async_computation.2 | async-start | bytes 6488064 | tf_op jit(solution)/shard_map/all_gather | solution.py:85
  8.0 307.6 %all-gather.9.cloned.1.call-start = ((), (), s32[]{:S(2)}) async-start(), calls=%async_computation.4 | async-start | bytes 6488064 | tf_op jit(solution)/shard_map/all_gather | solution.py:86
  9.2 66.1 %collective-permute-start.6 = (bf16[384,64]{0,1:T(8,128)(2,1)S(1)}, bf16[384,64]{0,1:T(8,128)(2,1)S(1)}, u32[]{:S(2)}, u32[]{:S(2)}) collective-permute-start(bf16[384,64]{0,1:T(8,128)(2,1)S(1)} %pad_maximum_fusion.4), channel_id=1, source_target_pairs={{0,12},{4,16},{8,20},{12,24},{16,28},{1,13},{5,17},{9,21},{13,25},... | collective-permute-start | bytes 147464 | tf_op jit(solution)/shard_map/ppermute | solution.py:21
  15.1 60.2 %collective-permute-start.7 = (bf16[384,64]{0,1:T(8,128)(2,1)S(1)}, bf16[384,64]{0,1:T(8,128)(2,1)S(1)}, u32[]{:S(2)}, u32[]{:S(2)}) collective-permute-start(bf16[384,64]{0,1:T(8,128)(2,1)S(1)} %pad_maximum_fusion.4), channel_id=1, source_target_pairs={{0,8},{4,12},{8,16},{12,20},{16,24},{20,28},{1,9},{5,13},{9,17},{1... | collective-permute-start | bytes 147464 | tf_op jit(solution)/shard_map/ppermute | solution.py:21
  18.6 8.0 %collective-permute-start.3 = (s32[384]{0:T(512)}, s32[384]{0:T(512)S(1)}, u32[]{:S(2)}, u32[]{:S(2)}) collective-permute-start(s32[384]{0:T(512)} %param.23), channel_id=1, source_target_pairs={{0,12},{4,16},{8,20},{12,24},{16,28},{1,13},{5,17},{9,21},{13,25},... | collective-permute-start | bytes 4616 | tf_op jit(solution)/shard_map/ppermute | solution.py:21
  21.5 7.7 %collective-permute-start.4 = (s32[384]{0:T(512)}, s32[384]{0:T(512)S(1)}, u32[]{:S(2)}, u32[]{:S(2)}) collective-permute-start(s32[384]{0:T(512)} %param.23), channel_id=1, source_target_pairs={{0,8},{4,12},{8,16},{12,20},{16,24},{20,28},{1,9},{5,13},{9,17},{1... | collective-permute-start | bytes 4616 | tf_op jit(solution)/shard_map/ppermute | solution.py:21
  23.4 7.1 %collective-permute-start.5 = (s32[384]{0:T(512)}, s32[384]{0:T(512)S(1)}, u32[]{:S(2)}, u32[]{:S(2)}) collective-permute-start(s32[384]{0:T(512)} %param.23), channel_id=1, source_target_pairs={{0,4},{4,8},{8,12},{12,16},{16,20},{20,24},{24,28},{1,5},{5,9},{9,... | collective-permute-start | bytes 4616 | tf_op jit(solution)/shard_map/ppermute | solution.py:21
  26.6 20.5 %collective-permute-start = (bf16[384,512]{1,0:T(8,128)(2,1)S(1)}, bf16[384,512]{1,0:T(8,128)(2,1)S(1)}, u32[]{:S(2)}, u32[]{:S(2)}) collective-permute-start(bf16[384,512]{1,0:T(8,128)(2,1)S(1)} %copy-done.5), channel_id=1, source_target_pairs={{0,12},{4,16},{8,20},{12,24},{16,28},{1,13},{5,17},{9,21},{13,25},... | collective-permute-start | bytes 1179656 | tf_op jit(solution)/shard_map/ppermute | solution.py:21
  29.2 32.3 %collective-permute-start.1 = (bf16[384,512]{1,0:T(8,128)(2,1)S(1)}, bf16[384,512]{1,0:T(8,128)(2,1)S(1)}, u32[]{:S(2)}, u32[]{:S(2)}) collective-permute-start(bf16[384,512]{1,0:T(8,128)(2,1)S(1)} %copy-done.5), channel_id=1, source_target_pairs={{0,8},{4,12},{8,16},{12,20},{16,24},{20,28},{1,9},{5,13},{9,17},{1... | collective-permute-start | bytes 1179656 | tf_op jit(solution)/shard_map/ppermute | solution.py:21
  30.5 31.0 %collective-permute-start.2 = (bf16[384,512]{1,0:T(8,128)(2,1)S(1)}, bf16[384,512]{1,0:T(8,128)(2,1)S(1)}, u32[]{:S(2)}, u32[]{:S(2)}) collective-permute-start(bf16[384,512]{1,0:T(8,128)(2,1)S(1)} %copy-done.5), channel_id=1, source_target_pairs={{0,4},{4,8},{8,12},{12,16},{16,20},{20,24},{24,28},{1,5},{5,9},{9,... | collective-permute-start | bytes 1179656 | tf_op jit(solution)/shard_map/ppermute | solution.py:21
  47.1 28.3 %collective-permute-start.8 = (bf16[384,64]{0,1:T(8,128)(2,1)S(1)}, bf16[384,64]{0,1:T(8,128)(2,1)S(1)}, u32[]{:S(2)}, u32[]{:S(2)}) collective-permute-start(bf16[384,64]{0,1:T(8,128)(2,1)S(1)} %pad_maximum_fusion.4), channel_id=1, source_target_pairs={{0,4},{4,8},{8,12},{12,16},{16,20},{20,24},{24,28},{1,5},{5,9},{9,... | collective-permute-start | bytes 147464 | tf_op jit(solution)/shard_map/ppermute | solution.py:21
  61.6 1.9 copy-start.4
  63.5 8.3 %copy-start.17 = (bf16[512,1024]{1,0:T(8,128)(2,1)S(1)}, bf16[512,1024]{1,0:T(8,128)(2,1)}, u32[]{:S(2)}) copy-start(bf16[512,1024]{1,0:T(8,128)(2,1)} %param.25) | copy-start | bytes 3145732
  125.9 16.3 %copy-start.10 = (bf16[512]{0:T(512)(128)(2,1)S(1)}, bf16[512]{0:T(512)(128)(2,1)}, u32[]{:S(2)}) copy-start(bf16[512]{0:T(512)(128)(2,1)} %param.27) | copy-start | bytes 3076
  125.9 16.3 %copy-start.11 = (bf16[512]{0:T(512)(128)(2,1)S(1)}, bf16[512]{0:T(512)(128)(2,1)}, u32[]{:S(2)}) copy-start(bf16[512]{0:T(512)(128)(2,1)} %param.28) | copy-start | bytes 3076
  125.9 16.3 %copy-start.8 = (bf16[3,1408]{1,0:T(4,128)(2,1)S(1)}, bf16[3,1408]{1,0:T(4,128)(2,1)}, u32[]{:S(2)}) copy-start(bf16[3,1408]{1,0:T(4,128)(2,1)} %param.31) | copy-start | bytes 25348
  125.9 16.3 %copy-start.9 = (bf16[3,1408]{1,0:T(4,128)(2,1)S(1)}, bf16[3,1408]{1,0:T(4,128)(2,1)}, u32[]{:S(2)}) copy-start(bf16[3,1408]{1,0:T(4,128)(2,1)} %param.32) | copy-start | bytes 25348
  125.9 24.0 %copy-start.3 = (bf16[384,512]{1,0:T(8,128)(2,1)S(1)}, bf16[384,512]{1,0:T(8,128)(2,1)}, u32[]{:S(2)}) copy-start(bf16[384,512]{1,0:T(8,128)(2,1)} %param.18) | copy-start | bytes 1179652
  125.9 23.7 %all-to-all-start = ((bf16[4,384,512]{2,1,0:T(8,128)(2,1)}), bf16[4,384,512]{2,1,0:T(8,128)(2,1)S(1)}, u32[]{:S(2)}, u32[]{:S(2)}) async-start(bf16[4,384,512]{2,1,0:T(8,128)(2,1)} %pad_maximum_fusion), calls=%async_computation | async-start | bytes 3145728 | tf_op jit(solution)/shard_map/all_to_all | solution.py:47
  129.7 13.7 %collective-permute-start.10 = (s32[2]{0:T(128)S(1)}, s32[2]{0:T(128)S(1)}, u32[]{:S(2)}, u32[]{:S(2)}) collective-permute-start(s32[2]{0:T(128)S(1)} %slice.108), channel_id=1, source_target_pairs={{0,4},{4,8},{8,12},{12,16},{16,20},{20,24},{24,28},{1,5},{5,9},{9,... | collective-permute-start | bytes 32 | tf_op jit(solution)/shard_map/ppermute | solution.py:21
  156.4 17.2 %copy-start.2 = (bf16[384,512]{1,0:T(8,128)(2,1)}, bf16[384,512]{1,0:T(8,128)(2,1)S(1)}, u32[]{:S(2)}) copy-start(bf16[384,512]{1,0:T(8,128)(2,1)S(1)} %add_convert_fusion.1) | copy-start | bytes 1179652
  178.9 1.0 copy-start.14
  180.0 144.1 %collective-permute-start.11 = (bf16[2,1408]{1,0:T(2,128)(2,1)S(1)}, bf16[2,1408]{1,0:T(2,128)(2,1)S(1)}, u32[]{:S(2)}, u32[]{:S(2)}) collective-permute-start(bf16[2,1408]{1,0:T(2,128)(2,1)S(1)} %slice.137), channel_id=1, source_target_pairs={{0,4},{4,8},{8,12},{12,16},{16,20},{20,24},{24,28},{1,5},{5,9},{9,... | collective-permute-start | bytes 16904 | tf_op jit(solution)/shard_map/ppermute | solution.py:21
  228.0 2.5 copy-start.16
  228.1 96.0 %collective-permute-start.9 = (bf16[2,1408]{1,0:T(2,128)(2,1)S(1)}, bf16[2,1408]{1,0:T(2,128)(2,1)S(1)}, u32[]{:S(2)}, u32[]{:S(2)}) collective-permute-start(bf16[2,1408]{1,0:T(2,128)(2,1)S(1)} %slice.134), channel_id=1, source_target_pairs={{0,4},{4,8},{8,12},{12,16},{16,20},{20,24},{24,28},{1,5},{5,9},{9,... | collective-permute-start | bytes 16904 | tf_op jit(solution)/shard_map/ppermute | solution.py:21
  315.7 8.4 %copy-start.15 = (bf16[384,1408]{1,0:T(8,128)(2,1)S(1)}, bf16[384,1408]{1,0:T(8,128)(2,1)}, u32[]{:S(2)}) copy-start(bf16[384,1408]{1,0:T(8,128)(2,1)} %copy-done.14) | copy-start | bytes 3244036
  335.0 3.7 copy-start.12
  335.0 3.7 copy-start.13
  335.0 23.7 %all-to-all-start.1 = ((bf16[4,384,512]{2,1,0:T(8,128)(2,1)}), bf16[4,384,512]{2,1,0:T(8,128)(2,1)S(1)}, u32[]{:S(2)}, u32[]{:S(2)}) async-start(bf16[4,384,512]{2,1,0:T(8,128)(2,1)} %pad_maximum_fusion.1), calls=%async_computation.1 | async-start | bytes 3145728 | tf_op jit(solution)/shard_map/all_to_all | solution.py:47
  338.7 29.2 %copy-start.1 = (bf16[512,1024]{1,0:T(8,128)(2,1)S(1)}, bf16[512,1024]{1,0:T(8,128)(2,1)}, u32[]{:S(2)}) copy-start(bf16[512,1024]{1,0:T(8,128)(2,1)} %param.24) | copy-start | bytes 3145732
Sparse Core Ops, SparseCore 0:
  9.5 118.1 all-gather.6
  129.9 92.8 all-gather.4
  225.0 90.6 all-gather.8
